TPU v7x, 32 devices: a whole 2x2x4 slice. The times are simulated.
32 devices in a mesh: fs: 8 (over z, y), tp: 4 (over x, core).
Axes of the slice: x: 2, y: 2, z: 4, core: 2. Of those that a mesh axis runs over, the one named last changes fastest.
Arguments:
- cotangent: bfloat16 [5120, 1024], P('fs', 'tp'), may hold values from -6 to 6
- inputs: bfloat16 [5120, 1024], P('fs', 'tp'), may hold values from -6 to 6
- pre_act: bfloat16 [5120, 2112], P('fs'), may hold values from -6 to 6
- w_up: bfloat16 [2112, 1024], P('fs', 'tp'), may hold values from -0.1875 to 0.1875
- w_down: bfloat16 [2112, 1024], P('fs', 'tp'), may hold values from -0.125 to 0.125
Outputs:
- grad_input: bfloat16 [5120, 1024], P('fs', 'tp')
- grad_up: float32 [2112, 1024], P('fs', 'tp')
All inputs are finite; a program needn't handle non-finite values.
Results may differ from a plain program's by a relative error of at most 0.0049.
Values may be sent and summed in bfloat16 or wider, within the bound.
A program may use at most 64 MiB of HBM per device.

v0:
```python
import jax
import jax.numpy as jnp
from jax import lax
from jax.sharding import PartitionSpec as P


def times_rows(left, piece):
    return lax.dot_general(
        left, piece, (((1,), (1,)), ((), ())), preferred_element_type=jnp.float32
    )


def local(cotangent, inputs, pre_act, w_up, w_down):
    row_count = cotangent.shape[0]
    token_total = row_count * lax.axis_size("fs")
    full_cotangent = lax.all_gather(cotangent, "tp", axis=1, tiled=True)
    down_whole = lax.all_gather(w_down, "tp", axis=1, tiled=True)
    grad_hidden = times_rows(full_cotangent, lax.all_gather(down_whole, "fs", axis=0, tiled=True))
    grad_pre = (2.0 * grad_hidden * jnp.maximum(pre_act.astype(jnp.float32), 0.0)).astype(
        jnp.bfloat16
    )
    columns = grad_pre
    grad_input = jnp.dot(
        columns, lax.all_gather(w_up, "fs", axis=0, tiled=True), preferred_element_type=jnp.float32
    )
    columns = grad_pre
    grad_share = lax.psum_scatter(
        lax.dot_general(
            columns, inputs, (((0,), (0,)), ((), ())), preferred_element_type=jnp.float32
        ),
        "fs",
        scatter_dimension=0,
        tiled=True,
    )
    grad_up = grad_share / jnp.sqrt(jnp.float32(token_total))
    return (grad_input.astype(jnp.bfloat16), grad_up)


def solution(mesh):
    return jax.shard_map(
        local,
        mesh=mesh,
        in_specs=(P("fs", "tp"), P("fs", "tp"), P("fs", None), P("fs", "tp"), P("fs", "tp")),
        out_specs=(P("fs", "tp"), P("fs", "tp")),
        check_vma=False,
    )
```

profile of v0, /device:TPU:0, one launch (start us, length us, event | category | flops | bytes accessed | tf_op | source)
XLA Modules:
  0.0 227.8 jit_solution(900045571831877215)
XLA Ops:
  7.2 0.0 copy-start
  7.2 0.0 all-gather.4.cloned.1.call-start
  7.2 0.7 all-gather.4.cloned.1.call-update
  7.9 0.0 all-gather.6.cloned.1.call-start
  8.0 10.3 %all_gather.13 = bf16[264,1024]{1,0:T(8,128)(2,1)} all-gather(bf16[264,256]{1,0:T(8,128)(2,1)} %param.9), channel_id=1, replica_groups=mesh['fs'=8,'tp'=4] {'tp'}, dimensions={1}, use_global_device_ids=true | all-gather | bytes 675840 | tf_op jit(solution)/shard_map/all_gather | solution.py:17
  18.3 0.0 all-gather.6.cloned.1.call-update
  18.3 0.0 all-gather.8.cloned.1.call-start
  18.4 0.7 all-gather.8.cloned.1.call-update
  19.1 0.0 reduce-scatter.2.cloned.1.call-start
  19.1 11.5 %all-gather.4.cloned.1.call-done = bf16[640,1024]{1,0:T(8,128)(2,1)} async-done(((bf16[640,256]{1,0:T(8,128)(2,1)}), bf16[640,1024]{1,0:T(8,128)(2,1)}) %all-gather.4.cloned.1.call-update) | async-done | bytes 1310736 | tf_op jit(solution)/shard_map/all_gather | solution.py:16
  30.6 76.6 %all-gather.6.cloned.1.call-done = bf16[2112,1024]{1,0:T(8,128)(2,1)} async-done(((bf16[264,1024]{1,0:T(8,128)(2,1)}), bf16[2112,1024]{1,0:T(8,128)(2,1)}) %all-gather.6.cloned.1.call-update) | async-done | bytes 4325392 | tf_op jit(solution)/shard_map/all_gather | solution.py:18
  107.2 7.1 %fusion.1 = bf16[640,2112]{0,1:T(8,128)(2,1)S(1)} fusion(bf16[640,2112]{0,1:T(8,128)(2,1)} %param.7, bf16[640,1024]{1,0:T(8,128)(2,1)} %all-gather.4.cloned.1.call-done, bf16[2112,1024]{1,0:T(8,128)(2,1)} %all-gather.6.cloned.1.call-done), kind=kOutput, calls=%fused_computation.2 | convolution fusion | flops 2774999040 | bytes 11042816 | tf_op jit(solution)/shard_map/dot_general | solution.py:8
  114.4 0.0 copy-done
  114.4 2.4 %fusion.2 = f32[2112,256]{1,0:T(8,128)} fusion(bf16[640,2112]{0,1:T(8,128)(2,1)S(1)} %fusion.1, bf16[640,256]{1,0:T(8,128)(2,1)S(1)} %copy-done), kind=kOutput, calls=%fused_computation.5 | convolution fusion | flops 692060160 | bytes 5193728 | tf_op jit(solution)/shard_map/dot_general | solution.py:28
  116.7 0.0 reduce-scatter.2.cloned.1.call-update
  116.8 31.7 %all-gather.8.cloned.1.call-done = bf16[2112,256]{1,0:T(8,128)(2,1)} async-done(((bf16[264,256]{1,0:T(8,128)(2,1)}), bf16[2112,256]{1,0:T(8,128)(2,1)}) %all-gather.8.cloned.1.call-update) | async-done | bytes 1081360 | tf_op jit(solution)/shard_map/all_gather | solution.py:24
  148.5 2.9 %convolution_convert_fusion = bf16[640,256]{1,0:T(8,128)(2,1)} fusion(bf16[640,2112]{0,1:T(8,128)(2,1)S(1)} %fusion.1, bf16[2112,256]{1,0:T(8,128)(2,1)} %all-gather.8.cloned.1.call-done), kind=kOutput, calls=%fused_computation.3 | convolution fusion | flops 692224000 | bytes 4112384 | tf_op jit(solution)/shard_map/dot_general | solution.py:23
  151.4 68.2 %reduce-scatter.2.cloned.1.call-done = f32[264,256]{1,0:T(8,128)} async-done(((f32[2112,256]{1,0:T(8,128)}), f32[264,256]{1,0:T(8,128)}) %reduce-scatter.2.cloned.1.call-update) | async-done | bytes 270352 | tf_op jit(solution)/shard_map/reduce_scatter | solution.py:27
  219.6 1.7 broadcast_multiply_fusion
Async XLA Ops:
  7.2 107.2 %copy-start = (bf16[640,256]{1,0:T(8,128)(2,1)S(1)}, bf16[640,256]{1,0:T(8,128)(2,1)}, u32[]{:S(2)}) copy-start(bf16[640,256]{1,0:T(8,128)(2,1)} %param.6) | copy-start | bytes 983044
  7.2 23.4 %all-gather.4.cloned.1.call-start = ((), (), s32[]{:S(2)}) async-start(), calls=%async_computation.1 | async-start | bytes 1638400 | tf_op jit(solution)/shard_map/all_gather | solution.py:16
  7.9 99.3 %all-gather.6.cloned.1.call-start = ((), (), s32[]{:S(2)}) async-start(), calls=%async_computation.2 | async-start | bytes 4866048 | tf_op jit(solution)/shard_map/all_gather | solution.py:18
  18.3 130.1 %all-gather.8.cloned.1.call-start = ((), (), s32[]{:S(2)}) async-start(), calls=%async_computation.3 | async-start | bytes 1216512 | tf_op jit(solution)/shard_map/all_gather | solution.py:24
  19.1 200.5 %reduce-scatter.2.cloned.1.call-start = ((), (), s32[]{:S(2)}) async-start(), calls=%async_computation.4 | async-start | bytes 2433024 | tf_op jit(solution)/shard_map/reduce_scatter | solution.py:27
Sparse Core Ops, SparseCore 0:
  9.5 21.0 all-gather.3
  32.8 74.3 all-gather.5
  109.4 39.0 all-gather.7
  151.8 67.7 reduce-scatter.1
where the time goes:
time: 228 us
  waiting for transfers between devices  189 us (83%)
  between operations  13.8 us (6%)
  matrix products  12.4 us (5%)
  blocking collectives  10.3 us (5%)
    all_gather x1, waiting for transfers between devices, local(): lax.all_gather(down_whole, 'fs', axis=0, tiled=True)  76.6 us
    reduce_scatter x1, waiting for transfers between devices, local(): lax.psum_scatter(lax.dot_general(columns, inputs, (((0,), (0,)), ((), ())...  68.2 us
    all_gather x1, waiting for transfers between devices, local(): lax.all_gather(w_up, 'fs', axis=0, tiled=True)  31.7 us
    all_gather x1, waiting for transfers between devices, local(): full_cotangent = lax.all_gather(cotangent, 'tp', axis=1, tiled=True)  11.5 us
    all_gather x1, blocking collectives, local(): down_whole = lax.all_gather(w_down, 'tp', axis=1, tiled=True)  10.3 us
    dot_general x1, matrix products, times_rows(): lax.dot_general(left, piece, (((1,), (1,)), ((), ())), preferred_element_...  7.12 us
  transfers between devices with their start and end apart: 4, of which 4 were waited for; matrix products, arithmetic and copies ran while one was open for 5% of the time, Pallas kernels for 0%

commit v1 on v0

v1 whole, which is shorter than its diff:
```python
import functools

import jax
import jax.numpy as jnp
from jax import lax
from jax.experimental import pallas as pl
from jax.experimental.pallas import tpu as pltpu
from jax.sharding import PartitionSpec as P

MESH = pl.DeviceIdType.MESH


def times_rows(left, piece):
    return lax.dot_general(
        left, piece, (((1,), (1,)), ((), ())), preferred_element_type=jnp.float32
    )


def toggled(index, mask, bits):
    for bit in range(bits):
        unit = 2**bit
        index = index + unit * ((mask // unit) % 2) * (1 - 2 * ((index // unit) % 2))
    return index


def kernel(
    n, token_total,
    cot_ref, in_ref, pre_ref, up_ref, down_ref,
    gi_ref, gu_ref,
    cot_buf, down_buf, up_buf, pre_buf, own_part, part_out, part_in,
    local_sem, cot_send, cot_recv, dz_send, dy_send, dx_send, dc_send, dr_send, down_recv,
    uz_send, uy_send, up_recv, part_send, part_recv,
):
    bits = n.bit_length() - 1
    half = n // 2
    f = lax.axis_index("fs")
    t = lax.axis_index("tp")
    width = cot_ref.shape[1]
    rows = down_ref.shape[0]
    t_core = toggled(t, 1, 2)
    t_x = toggled(t, 2, 2)
    t_xcore = toggled(t, 3, 2)

    def seq(i):
        return toggled(f, i, bits)

    def cols(tp):
        return pl.ds(pl.multiple_of(tp * width, width), width)

    def down_slot(src_f, src_t):
        return down_buf.at[src_f, :, cols(src_t)]

    def remote(src, dst, send, recv, fs, tp):
        return pltpu.make_async_remote_copy(
            src_ref=src, dst_ref=dst, send_sem=send, recv_sem=recv,
            device_id=(fs, tp), device_id_type=MESH,
        )

    barrier = pltpu.get_barrier_semaphore()
    peers = [(seq(i), t) for i in range(1, n)] + [(f, t_core), (f, t_x)]
    for peer in peers:
        pl.semaphore_signal(barrier, inc=1, device_id=peer, device_id_type=MESH)
    pl.semaphore_wait(barrier, len(peers))

    def cot_copy(src, src_t, slot, tp):
        return remote(src, cot_buf.at[:, cols(src_t)], cot_send.at[slot], cot_recv.at[src_t], f, tp)

    def down_copy(src, src_f, src_t, send, fs, tp):
        return remote(src, down_slot(src_f, src_t), send, down_recv.at[src_f, src_t], fs, tp)

    def up_copy(src, src_f, send, fs):
        return remote(src, up_buf.at[src_f], send, up_recv.at[src_f], fs, t)

    sent = []

    def go(copy):
        copy.start()
        sent.append(copy)

    go(cot_copy(cot_ref, t, 0, t_core))
    go(cot_copy(cot_ref, t, 1, t_x))
    for k in range(1, half):
        go(down_copy(down_ref, f, t, dz_send.at[k], seq(2 * k), t))
    go(down_copy(down_ref, f, t, dy_send.at[0], seq(1), t))
    go(down_copy(down_ref, f, t, dx_send.at[0], f, t_x))
    go(down_copy(down_ref, f, t, dc_send.at[0], f, t_core))
    for k in range(1, half):
        go(up_copy(up_ref, f, uz_send.at[k], seq(2 * k)))
    go(up_copy(up_ref, f, uy_send.at[0], seq(1)))

    local = [
        pltpu.make_async_copy(cot_ref, cot_buf.at[:, cols(t)], local_sem.at[0]),
        pltpu.make_async_copy(down_ref, down_slot(f, t), local_sem.at[1]),
        pltpu.make_async_copy(up_ref, up_buf.at[f], local_sem.at[2]),
    ]
    for copy in local:
        copy.start()

    for block in range(n):
        pre_buf[block] = pre_ref[:, block * rows : (block + 1) * rows]

    def arrived_down(src_f, src_t):
        down_copy(down_slot(src_f, src_t), src_f, src_t, dz_send.at[0], f, t_core).wait_recv()

    def arrived_up(src_f):
        up_copy(up_buf.at[src_f], src_f, uz_send.at[0], seq(1)).wait_recv()

    def arrived_cot(src_t):
        cot_copy(cot_buf.at[:, cols(src_t)], src_t, 0, t_core).wait_recv()

    def take_own(i):
        src = seq(i)
        arrived_down(src, t)
        block = down_slot(src, t)
        down_copy(block, src, t, dx_send.at[i], f, t_x).start()
        down_copy(block, src, t, dc_send.at[i], f, t_core).start()

        @pl.when(i % 2 == 0)
        def _():
            down_copy(block, src, t, dy_send.at[i // 2], seq(1), t).start()

    for copy in local:
        copy.wait()
    take_own(1)
    arrived_cot(t_x)
    go(cot_copy(cot_buf.at[:, cols(t_x)], t_x, 2, t_core))
    arrived_cot(t_core)
    arrived_cot(t_xcore)

    def step(i, carry):
        @pl.when(i < n - 2)
        def _():
            take_own(i + 2)

        @pl.when(i < n)
        def _():
            src = seq(i)
            arrived_down(src, t_x)
            down_copy(down_slot(src, t_x), src, t_x, dr_send.at[i], f, t_core).start()

            @pl.when((i % 2 == 0) & (i > 0))
            def _():
                arrived_up(src)
                up_copy(up_buf.at[src], src, uy_send.at[i // 2], seq(1)).start()

        @pl.when(i > 0)
        def _():
            j = i - 1
            src = seq(j)
            arrived_down(src, t_core)
            arrived_down(src, t_xcore)
            hidden = times_rows(cot_buf[...], down_buf[src])
            grad_pre = (
                2.0 * hidden * jnp.maximum(pre_buf[src].astype(jnp.float32), 0.0)
            ).astype(jnp.bfloat16)
            pre_buf[src] = grad_pre
            part = lax.dot_general(
                grad_pre, in_ref[...], (((0,), (0,)), ((), ())), preferred_element_type=jnp.float32
            )

            @pl.when(j == 0)
            def _():
                own_part[...] = part

            @pl.when(j > 0)
            def _():
                part_out[j] = part.astype(jnp.bfloat16)
                remote(part_out.at[j], part_in.at[f], part_send.at[j], part_recv.at[f], src, t).start()

        return carry

    lax.fori_loop(0, n + 1, step, 0)

    for i in range(1, n, 2):
        arrived_up(seq(i))
    gi = jnp.zeros(gi_ref.shape, jnp.float32)
    for block in range(n):
        gi = gi + jnp.dot(pre_buf[block], up_buf[block], preferred_element_type=jnp.float32)
    gi_ref[...] = gi.astype(gi_ref.dtype)

    total = own_part[...]
    for i in range(1, n):
        src = seq(i)
        remote(part_out.at[i], part_in.at[src], part_send.at[i], part_recv.at[src], src, t).wait_recv()
        total = total + part_in[src].astype(jnp.float32)
    gu_ref[...] = total / jnp.sqrt(jnp.float32(token_total))

    for copy in sent:
        copy.wait_send()
    for i in range(1, n):
        src = seq(i)
        block = down_slot(src, t)
        down_copy(block, src, t, dx_send.at[i], f, t_x).wait_send()
        down_copy(block, src, t, dc_send.at[i], f, t_core).wait_send()
        remote(part_out.at[i], part_in.at[f], part_send.at[i], part_recv.at[f], src, t).wait_send()
        if i % 2 == 0:
            down_copy(block, src, t, dy_send.at[i // 2], seq(1), t).wait_send()
            up_copy(up_buf.at[src], src, uy_send.at[i // 2], seq(1)).wait_send()
    for i in range(n):
        src = seq(i)
        down_copy(down_slot(src, t_x), src, t_x, dr_send.at[i], f, t_core).wait_send()


def fused(n, tp, cotangent, inputs, pre_act, w_up, w_down):
    tokens, width = cotangent.shape
    rows = w_down.shape[0]
    dma = pltpu.SemaphoreType.DMA
    half = n // 2
    return pl.pallas_call(
        functools.partial(kernel, n, tokens * n),
        out_shape=(
            jax.ShapeDtypeStruct((tokens, width), jnp.bfloat16),
            jax.ShapeDtypeStruct((rows, width), jnp.float32),
        ),
        in_specs=[pl.BlockSpec(memory_space=pltpu.VMEM)] * 5,
        out_specs=(pl.BlockSpec(memory_space=pltpu.VMEM),) * 2,
        scratch_shapes=[
            pltpu.VMEM((tokens, tp * width), jnp.bfloat16),
            pltpu.VMEM((n, rows, tp * width), jnp.bfloat16),
            pltpu.VMEM((n, rows, width), jnp.bfloat16),
            pltpu.VMEM((n, tokens, rows), jnp.bfloat16),
            pltpu.VMEM((rows, width), jnp.float32),
            pltpu.VMEM((n, rows, width), jnp.bfloat16),
            pltpu.VMEM((n, rows, width), jnp.bfloat16),
            dma((3,)),
            dma((3,)), dma((tp,)),
            dma((half,)), dma((half,)), dma((n,)), dma((n,)), dma((n,)), dma((n, tp)),
            dma((half,)), dma((half,)), dma((n,)),
            dma((n,)), dma((n,)),
        ],
        compiler_params=pltpu.CompilerParams(
            collective_id=0, has_side_effects=True, vmem_limit_bytes=60 * 2**20
        ),
    )(cotangent, inputs, pre_act, w_up, w_down)


def gathered(cotangent, inputs, pre_act, w_up, w_down):
    token_total = cotangent.shape[0] * lax.axis_size("fs")
    full_cotangent = lax.all_gather(cotangent, "tp", axis=1, tiled=True)
    down_whole = lax.all_gather(w_down, "tp", axis=1, tiled=True)
    grad_hidden = times_rows(full_cotangent, lax.all_gather(down_whole, "fs", axis=0, tiled=True))
    grad_pre = (2.0 * grad_hidden * jnp.maximum(pre_act.astype(jnp.float32), 0.0)).astype(
        jnp.bfloat16
    )
    grad_input = jnp.dot(
        grad_pre, lax.all_gather(w_up, "fs", axis=0, tiled=True), preferred_element_type=jnp.float32
    )
    grad_share = lax.psum_scatter(
        lax.dot_general(
            grad_pre, inputs, (((0,), (0,)), ((), ())), preferred_element_type=jnp.float32
        ),
        "fs",
        scatter_dimension=0,
        tiled=True,
    )
    grad_up = grad_share / jnp.sqrt(jnp.float32(token_total))
    return (grad_input.astype(jnp.bfloat16), grad_up)


def solution(mesh):
    n, tp = mesh.shape["fs"], mesh.shape["tp"]

    def local(cotangent, inputs, pre_act, w_up, w_down):
        rows, width = w_down.shape
        fits = tp == 4 and 4 <= n <= 16 and n & (n - 1) == 0 and rows % 8 == 0 and width % 128 == 0
        if fits:
            return fused(n, tp, cotangent, inputs, pre_act, w_up, w_down)
        return gathered(cotangent, inputs, pre_act, w_up, w_down)

    return jax.shard_map(
        local,
        mesh=mesh,
        in_specs=(P("fs", "tp"), P("fs", "tp"), P("fs", None), P("fs", "tp"), P("fs", "tp")),
        out_specs=(P("fs", "tp"), P("fs", "tp")),
        check_vma=False,
    )
```

time: 228 us -> 76 us (0.33)
  the two profiles are of different devices: /device:TPU:0 before, /device:TPU:13 now
where the time goes in v1:
time: 76 us; the launch traced here: 75.7 us
  Pallas kernels  66.4 us (87%)
  local copies, waits for them, and re-layouts  8.73 us (11%)
    pallas_call x1, Pallas kernels, fused(): pl.pallas_call(functools.partial(kernel, n, tokens * n), out_shape=(jax.S...  66.4 us
    unnamed x3, local copies, waits for them, and re-layouts  8.73 us

profile of v1, /device:TPU:13, one launch (start us, length us, event | category | flops | bytes accessed | tf_op | source)
XLA Modules:
  0.0 75.7 jit_solution(302366266432484228)
XLA Ops:
  0.6 5.3 %copy.7.pre_ref = bf16[640,2112]{1,0:T(8,128)(2,1)} copy(bf16[640,2112]{0,1:T(8,128)(2,1)} %param.7) | data formatting | bytes 5406720 | tf_op args[2]
  6.0 66.4 %shard_map.68 = (bf16[640,256]{1,0:T(8,128)(2,1)}, f32[264,256]{1,0:T(8,128)}) custom-call(bf16[640,256]{1,0:T(8,128)(2,1)} %cot_ref.1, bf16[640,256]{1,0:T(8,128)(2,1)} %in_ref.1, bf16[640,2112]{1,0:T(8,128)(2,1)} %copy.7.pre_ref, bf16[264,256]{1,0:T(8,128)(2,1)} %up_ref.1, bf16[264,256]{1,0:T(8,128)(2,1)} %down_ref.1), custom_call_target="tpu_custom_call" | custom-call | tf_op jit(solution)/shard_map/pallas_call | solution.py:209
  72.3 1.7 %copy.10 = bf16[640,256]{1,0:T(8,128)(2,1)} copy(bf16[640,256]{1,0:T(8,128)(2,1)} %get-tuple-element.4) | data formatting | bytes 655360
  74.1 1.7 %copy.11 = f32[264,256]{1,0:T(8,128)} copy(f32[264,256]{1,0:T(8,128)} %get-tuple-element.5) | data formatting | bytes 540672

commit v2 on v1

v2 whole, which is shorter than its diff:
```python
import functools

import jax
import jax.numpy as jnp
from jax import lax
from jax.experimental import pallas as pl
from jax.experimental.pallas import tpu as pltpu
from jax.sharding import PartitionSpec as P

MESH = pl.DeviceIdType.MESH


def times_rows(left, piece):
    return lax.dot_general(
        left, piece, (((1,), (1,)), ((), ())), preferred_element_type=jnp.float32
    )


def toggled(index, mask, bits):
    for bit in range(bits):
        unit = 2**bit
        index = index + unit * ((mask // unit) % 2) * (1 - 2 * ((index // unit) % 2))
    return index


def kernel(
    n, token_total,
    cot_ref, in_ref, pre_ref, up_ref, down_ref,
    gi_ref, gu_ref,
    cot_buf, cot_turned, down_buf, up_buf, pre_buf, held, y_out, y_in, z_out, z_in,
    local_sem, cot_send, cot_recv, dz_send, dy_send, dx_send, dc_send, dr_send, down_recv,
    uz_send, uy_send, up_recv, ys_send, ys_recv, zs_send, zs_recv,
):
    bits = n.bit_length() - 1
    half = n // 2
    f = lax.axis_index("fs")
    t = lax.axis_index("tp")
    width = cot_ref.shape[1]
    t_core = toggled(t, 1, 2)
    t_x = toggled(t, 2, 2)
    t_xcore = toggled(t, 3, 2)
    f_y = toggled(f, 1, 1)

    def split(i):
        pair = i // 2
        last = pair // (half - 1)
        return (pair + 1) % half, i % 2 + last * (1 - 2 * (i % 2))

    def seq(i):
        far, across = split(i)
        return toggled(f, 2 * far + across, bits)

    def cols(tp):
        return pl.ds(pl.multiple_of(tp * width, width), width)

    def down_slot(src_f, src_t):
        return down_buf.at[src_f, :, cols(src_t)]

    def remote(src, dst, send, recv, fs, tp):
        return pltpu.make_async_remote_copy(
            src_ref=src, dst_ref=dst, send_sem=send, recv_sem=recv,
            device_id=(fs, tp), device_id_type=MESH,
        )

    def cot_copy(src, src_t, slot, tp):
        return remote(src, cot_buf.at[:, cols(src_t)], cot_send.at[slot], cot_recv.at[src_t], f, tp)

    def down_copy(src, src_f, src_t, send, fs, tp):
        return remote(src, down_slot(src_f, src_t), send, down_recv.at[src_f, src_t], fs, tp)

    def up_copy(src, src_f, send, fs):
        return remote(src, up_buf.at[src_f], send, up_recv.at[src_f], fs, t)

    def y_copy(pair):
        return remote(y_out.at[pair], y_in.at[pair], ys_send.at[pair], ys_recv.at[pair], f_y, t)

    def z_copy(pair):
        owner = toggled(f, 2 * (pair + 1), bits)
        return remote(z_out.at[pair], z_in.at[pair], zs_send.at[pair], zs_recv.at[pair], owner, t)

    local = [
        pltpu.make_async_copy(cot_ref, cot_buf.at[:, cols(t)], local_sem.at[0]),
        pltpu.make_async_copy(down_ref, down_slot(f, t), local_sem.at[1]),
        pltpu.make_async_copy(up_ref, up_buf.at[f], local_sem.at[2]),
        pltpu.make_async_copy(pre_ref, pre_buf, local_sem.at[3]),
    ]
    for copy in local:
        copy.start()

    barrier = pltpu.get_barrier_semaphore()
    far_peers = [toggled(f, 2 * k, bits) for k in range(1, half)]
    peers = [(peer, t) for peer in far_peers] + [(f_y, t), (f, t_core), (f, t_x)]
    for peer in peers:
        pl.semaphore_signal(barrier, inc=1, device_id=peer, device_id_type=MESH)
    pl.semaphore_wait(barrier, len(peers))

    sent = []

    def go(copy):
        copy.start()
        sent.append(copy)

    go(cot_copy(cot_ref, t, 1, t_x))
    for k in range(1, half):
        go(down_copy(down_ref, f, t, dz_send.at[k], far_peers[k - 1], t))
    go(down_copy(down_ref, f, t, dy_send.at[0], f_y, t))
    go(cot_copy(cot_ref, t, 0, t_core))
    for k in range(1, half):
        go(up_copy(up_ref, f, uz_send.at[k], far_peers[k - 1]))

    def arrived_down(src_f, src_t):
        down_copy(down_slot(src_f, src_t), src_f, src_t, dz_send.at[0], f, t_core).wait_recv()

    def arrived_up(src_f):
        up_copy(up_buf.at[src_f], src_f, uz_send.at[0], f_y).wait_recv()

    def arrived_cot(src_t):
        cot_copy(cot_buf.at[:, cols(src_t)], src_t, 0, t_core).wait_recv()

    def take_own(i):
        far, across = split(i)
        src = seq(i)

        @pl.when(far + across > 0)
        def _():
            arrived_down(src, t)

        block = down_slot(src, t)
        down_copy(block, src, t, dx_send.at[i], f, t_x).start()
        down_copy(block, src, t, dc_send.at[i], f, t_core).start()

        @pl.when((far > 0) & (across == 0))
        def _():
            down_copy(block, src, t, dy_send.at[far], f_y, t).start()

    local[1].wait()
    take_own(0)
    arrived_cot(t_x)
    go(cot_copy(cot_buf.at[:, cols(t_x)], t_x, 2, t_core))
    take_own(1)
    go(up_copy(up_ref, f, uy_send.at[0], f_y))
    local[0].wait()
    arrived_cot(t_core)
    arrived_cot(t_xcore)
    cot_turned[...] = cot_buf[...].T
    local[2].wait()
    local[3].wait()

    def step(i, carry):
        @pl.when(i < n - 2)
        def _():
            take_own(i + 2)

        @pl.when(i < n)
        def _():
            src = seq(i)
            arrived_down(src, t_x)
            down_copy(down_slot(src, t_x), src, t_x, dr_send.at[i], f, t_core).start()

        @pl.when((i >= 3) & (i < half + 2))
        def _():
            k = i - 2
            src = toggled(f, 2 * k, bits)
            arrived_up(src)
            up_copy(up_buf.at[src], src, uy_send.at[k], f_y).start()

        @pl.when((i >= 4) & (i % 2 == 0))
        def _():
            pair = i // 2 - 2
            y_copy(pair).wait_recv()
            z_out[pair] = (held[pair] + y_in[pair].astype(jnp.float32)).astype(jnp.bfloat16)
            z_copy(pair).start()

        @pl.when(i > 0)
        def _():
            j = i - 1
            src = seq(j)
            pair = j // 2
            arrived_down(src, t_core)
            arrived_down(src, t_xcore)
            hidden = jnp.dot(down_buf[src], cot_turned[...], preferred_element_type=jnp.float32)
            grad_pre = (
                2.0 * hidden * jnp.maximum(pre_buf[src].astype(jnp.float32), 0.0)
            ).astype(jnp.bfloat16)
            pre_buf[src] = grad_pre
            part = jnp.dot(grad_pre, in_ref[...], preferred_element_type=jnp.float32)
            _, across = split(j)

            @pl.when(across == 0)
            def _():
                held[pair] = part

            @pl.when(across == 1)
            def _():
                y_out[pair] = part.astype(jnp.bfloat16)
                y_copy(pair).start()

        return carry

    lax.fori_loop(0, n + 1, step, 0)

    for k in range(half):
        arrived_up(toggled(f, 2 * k + 1, bits))
    gi = jnp.zeros(gi_ref.shape, jnp.float32)
    for block in range(n):
        gi = gi + lax.dot_general(
            pre_buf[block], up_buf[block], (((0,), (0,)), ((), ())),
            preferred_element_type=jnp.float32,
        )
    gi_ref[...] = gi.astype(gi_ref.dtype)

    total = held[half - 1]
    for pair in range(half - 1):
        z_copy(pair).wait_recv()
        total = total + z_in[pair].astype(jnp.float32)
    y_copy(half - 1).wait_recv()
    total = total + y_in[half - 1].astype(jnp.float32)
    gu_ref[...] = total / jnp.sqrt(jnp.float32(token_total))

    for copy in sent:
        copy.wait_send()
    for i in range(n):
        src = seq(i)
        far, across = split(i)
        block = down_slot(src, t)
        down_copy(block, src, t, dx_send.at[i], f, t_x).wait_send()
        down_copy(block, src, t, dc_send.at[i], f, t_core).wait_send()
        down_copy(down_slot(src, t_x), src, t_x, dr_send.at[i], f, t_core).wait_send()
        if far > 0 and across == 0:
            down_copy(block, src, t, dy_send.at[far], f_y, t).wait_send()
            up_copy(up_buf.at[src], src, uy_send.at[far], f_y).wait_send()
    for pair in range(half):
        y_copy(pair).wait_send()
        if pair < half - 1:
            z_copy(pair).wait_send()


def fused(n, tp, cotangent, inputs, pre_act, w_up, w_down):
    tokens, width = cotangent.shape
    rows = w_down.shape[0]
    dma = pltpu.SemaphoreType.DMA
    half = n // 2
    vmem = pl.BlockSpec(memory_space=pltpu.VMEM)
    return pl.pallas_call(
        functools.partial(kernel, n, tokens * n),
        out_shape=(
            jax.ShapeDtypeStruct((tokens, width), jnp.bfloat16),
            jax.ShapeDtypeStruct((rows, width), jnp.float32),
        ),
        in_specs=[vmem, vmem, pl.BlockSpec(memory_space=pl.ANY), vmem, vmem],
        out_specs=(vmem, vmem),
        scratch_shapes=[
            pltpu.VMEM((tokens, tp * width), jnp.bfloat16),
            pltpu.VMEM((tp * width, tokens), jnp.bfloat16),
            pltpu.VMEM((n, rows, tp * width), jnp.bfloat16),
            pltpu.VMEM((n, rows, width), jnp.bfloat16),
            pltpu.VMEM((n, rows, tokens), jnp.bfloat16),
            pltpu.VMEM((half, rows, width), jnp.float32),
            pltpu.VMEM((half, rows, width), jnp.bfloat16),
            pltpu.VMEM((half, rows, width), jnp.bfloat16),
            pltpu.VMEM((half - 1, rows, width), jnp.bfloat16),
            pltpu.VMEM((half - 1, rows, width), jnp.bfloat16),
            dma((4,)),
            dma((3,)), dma((tp,)),
            dma((half,)), dma((half,)), dma((n,)), dma((n,)), dma((n,)), dma((n, tp)),
            dma((half,)), dma((half,)), dma((n,)),
            dma((half,)), dma((half,)), dma((half - 1,)), dma((half - 1,)),
        ],
        compiler_params=pltpu.CompilerParams(
            collective_id=0, has_side_effects=True, vmem_limit_bytes=60 * 2**20
        ),
    )(cotangent, inputs, pre_act.T.reshape(n, rows, tokens), w_up, w_down)


def gathered(cotangent, inputs, pre_act, w_up, w_down):
    token_total = cotangent.shape[0] * lax.axis_size("fs")
    full_cotangent = lax.all_gather(cotangent, "tp", axis=1, tiled=True)
    down_whole = lax.all_gather(w_down, "tp", axis=1, tiled=True)
    grad_hidden = times_rows(full_cotangent, lax.all_gather(down_whole, "fs", axis=0, tiled=True))
    grad_pre = (2.0 * grad_hidden * jnp.maximum(pre_act.astype(jnp.float32), 0.0)).astype(
        jnp.bfloat16
    )
    grad_input = jnp.dot(
        grad_pre, lax.all_gather(w_up, "fs", axis=0, tiled=True), preferred_element_type=jnp.float32
    )
    grad_share = lax.psum_scatter(
        lax.dot_general(
            grad_pre, inputs, (((0,), (0,)), ((), ())), preferred_element_type=jnp.float32
        ),
        "fs",
        scatter_dimension=0,
        tiled=True,
    )
    grad_up = grad_share / jnp.sqrt(jnp.float32(token_total))
    return (grad_input.astype(jnp.bfloat16), grad_up)


def solution(mesh):
    n, tp = mesh.shape["fs"], mesh.shape["tp"]

    def local(cotangent, inputs, pre_act, w_up, w_down):
        rows, width = w_down.shape
        fits = tp == 4 and 4 <= n <= 16 and n & (n - 1) == 0 and rows % 8 == 0 and width % 128 == 0
        if fits:
            return fused(n, tp, cotangent, inputs, pre_act, w_up, w_down)
        return gathered(cotangent, inputs, pre_act, w_up, w_down)

    return jax.shard_map(
        local,
        mesh=mesh,
        in_specs=(P("fs", "tp"), P("fs", "tp"), P("fs", None), P("fs", "tp"), P("fs", "tp")),
        out_specs=(P("fs", "tp"), P("fs", "tp")),
        check_vma=False,
    )
```

time: 76 us -> 60.3 us (0.79)
  the two profiles are of different devices: /device:TPU:13 before, /device:TPU:0 now
where the time goes in v2:
time: 60.3 us; the launch traced here: 60.1 us
  Pallas kernels  56.1 us (93%)
  local copies, waits for them, and re-layouts  3.39 us (6%)
  between operations  0.64 us (1%)
    pallas_call x1, Pallas kernels, fused(): pl.pallas_call(functools.partial(kernel, n, tokens * n), out_shape=(jax.S...  56.1 us
    unnamed x2, local copies, waits for them, and re-layouts  3.39 us

profile of v2, /device:TPU:0, one launch (start us, length us, event | category | flops | bytes accessed | tf_op | source)
XLA Modules:
  0.0 60.1 jit_solution(10632798403142279164)
XLA Ops:
  0.6 56.1 %shard_map.68 = (bf16[640,256]{1,0:T(8,128)(2,1)}, f32[264,256]{1,0:T(8,128)}) custom-call(bf16[640,256]{1,0:T(8,128)(2,1)} %cot_ref.1, bf16[640,256]{1,0:T(8,128)(2,1)} %in_ref.1, bf16[8,264,640]{2,1,0:T(8,128)(2,1)} %bitcast.3, bf16[264,256]{1,0:T(8,128)(2,1)} %up_ref.1, bf16[264,256]{1,0:T(8,128)(2,1)} %down_ref.1), custom_call_target="tpu_custom_call" | custom-call | tf_op jit(solution)/shard_map/pallas_call | solution.py:244
  56.7 1.7 %copy.9 = bf16[640,256]{1,0:T(8,128)(2,1)} copy(bf16[640,256]{1,0:T(8,128)(2,1)} %get-tuple-element.4) | data formatting | bytes 655360
  58.4 1.7 %copy.10 = f32[264,256]{1,0:T(8,128)} copy(f32[264,256]{1,0:T(8,128)} %get-tuple-element.5) | data formatting | bytes 540672

commit v3 on v2

--- a/solution.py
+++ b/solution.py
@@ -105,8 +105,6 @@
         go(down_copy(down_ref, f, t, dz_send.at[k], far_peers[k - 1], t))
     go(down_copy(down_ref, f, t, dy_send.at[0], f_y, t))
     go(cot_copy(cot_ref, t, 0, t_core))
-    for k in range(1, half):
-        go(up_copy(up_ref, f, uz_send.at[k], far_peers[k - 1]))
 
     def arrived_down(src_f, src_t):
         down_copy(down_slot(src_f, src_t), src_f, src_t, dz_send.at[0], f, t_core).wait_recv()
@@ -138,6 +136,8 @@
     arrived_cot(t_x)
     go(cot_copy(cot_buf.at[:, cols(t_x)], t_x, 2, t_core))
     take_own(1)
+    for k in range(1, half):
+        go(up_copy(up_ref, f, uz_send.at[k], far_peers[k - 1]))
     go(up_copy(up_ref, f, uy_send.at[0], f_y))
     local[0].wait()
     arrived_cot(t_core)
@@ -147,9 +147,9 @@
     local[3].wait()
 
     def step(i, carry):
-        @pl.when(i < n - 2)
-        def _():
-            take_own(i + 2)
+        @pl.when((i < n - 1) & (i > 0))
+        def _():
+            take_own(i + 1)
 
         @pl.when(i < n)
         def _():
@@ -163,13 +163,6 @@
             src = toggled(f, 2 * k, bits)
             arrived_up(src)
             up_copy(up_buf.at[src], src, uy_send.at[k], f_y).start()
-
-        @pl.when((i >= 4) & (i % 2 == 0))
-        def _():
-            pair = i // 2 - 2
-            y_copy(pair).wait_recv()
-            z_out[pair] = (held[pair] + y_in[pair].astype(jnp.float32)).astype(jnp.bfloat16)
-            z_copy(pair).start()
 
         @pl.when(i > 0)
         def _():
@@ -194,6 +187,13 @@
             def _():
                 y_out[pair] = part.astype(jnp.bfloat16)
                 y_copy(pair).start()
+
+        @pl.when((i >= 3) & (i % 2 == 1))
+        def _():
+            pair = (i - 3) // 2
+            y_copy(pair).wait_recv()
+            z_out[pair] = (held[pair] + y_in[pair].astype(jnp.float32)).astype(jnp.bfloat16)
+            z_copy(pair).start()
 
         return carry
 
@@ -235,18 +235,24 @@
             z_copy(pair).wait_send()
 
 
+def settle(gi_ref, gu_ref, gi_out, gu_out):
+    gi_out[...] = gi_ref[...]
+    gu_out[...] = gu_ref[...]
+
+
 def fused(n, tp, cotangent, inputs, pre_act, w_up, w_down):
     tokens, width = cotangent.shape
     rows = w_down.shape[0]
     dma = pltpu.SemaphoreType.DMA
     half = n // 2
     vmem = pl.BlockSpec(memory_space=pltpu.VMEM)
-    return pl.pallas_call(
+    shapes = (
+        jax.ShapeDtypeStruct((tokens, width), jnp.bfloat16),
+        jax.ShapeDtypeStruct((rows, width), jnp.float32),
+    )
+    results = pl.pallas_call(
         functools.partial(kernel, n, tokens * n),
-        out_shape=(
-            jax.ShapeDtypeStruct((tokens, width), jnp.bfloat16),
-            jax.ShapeDtypeStruct((rows, width), jnp.float32),
-        ),
+        out_shape=shapes,
         in_specs=[vmem, vmem, pl.BlockSpec(memory_space=pl.ANY), vmem, vmem],
         out_specs=(vmem, vmem),
         scratch_shapes=[
@@ -270,6 +276,9 @@
             collective_id=0, has_side_effects=True, vmem_limit_bytes=60 * 2**20
         ),
     )(cotangent, inputs, pre_act.T.reshape(n, rows, tokens), w_up, w_down)
+    return pl.pallas_call(
+        settle, out_shape=shapes, in_specs=[vmem, vmem], out_specs=(vmem, vmem)
+    )(*results)
 
 
 def gathered(cotangent, inputs, pre_act, w_up, w_down):

time: 60.3 us -> 56.9 us (0.944)
  local copies, waits for them, and re-layouts: 3.39 us -> 0 us
    unnamed x2 -> x0, local copies, waits for them, and re-layouts: 3.39 us -> none
    pallas_call x1 -> x2, Pallas kernels: 56.1 us -> 56.1 us  [the longest x1 54.2 us: fused(): pl.pallas_call(functools.partial(kernel, n, tokens * n), out_shape=shapes...]
where the time goes in v3:
time: 56.9 us; the launch traced here: 56.7 us
  Pallas kernels  56.1 us (99%)
  between operations  0.64 us (1%)
    pallas_call x1, Pallas kernels, fused(): pl.pallas_call(functools.partial(kernel, n, tokens * n), out_shape=shapes...  54.2 us
    pallas_call x1, Pallas kernels, fused(): pl.pallas_call(settle, out_shape=shapes, in_specs=[vmem, vmem], out_specs...  1.89 us

profile of v3, /device:TPU:0, one launch (start us, length us, event | category | flops | bytes accessed | tf_op | source)
XLA Modules:
  0.0 56.7 jit_solution(11735716505512569928)
XLA Ops:
  0.6 54.2 %shard_map.68 = (bf16[640,256]{1,0:T(8,128)(2,1)}, f32[264,256]{1,0:T(8,128)}) custom-call(bf16[640,256]{1,0:T(8,128)(2,1)} %cot_ref.1, bf16[640,256]{1,0:T(8,128)(2,1)} %in_ref.1, bf16[8,264,640]{2,1,0:T(8,128)(2,1)} %bitcast.3, bf16[264,256]{1,0:T(8,128)(2,1)} %up_ref.1, bf16[264,256]{1,0:T(8,128)(2,1)} %down_ref.1), custom_call_target="tpu_custom_call" | custom-call | tf_op jit(solution)/shard_map/pallas_call | solution.py:253
  54.9 1.9 %shard_map.69 = (bf16[640,256]{1,0:T(8,128)(2,1)}, f32[264,256]{1,0:T(8,128)}) custom-call(bf16[640,256]{1,0:T(8,128)(2,1)} %get-tuple-element.4.gi_ref, f32[264,256]{1,0:T(8,128)} %get-tuple-element.5.gu_ref), custom_call_target="tpu_custom_call" | custom-call | tf_op jit(solution)/shard_map/pallas_call | solution.py:279
